TPU v7x, 32 devices: a whole 2x2x4 slice. The times are simulated.
32 devices in a mesh: sp: 16 (over z, y, x), tp: 2 (over core).
Axes of the slice: x: 2, y: 2, z: 4, core: 2. Of those that a mesh axis runs over, the one named last changes fastest.
Arguments:
- cotangent: bfloat16 [3072, 2048], P('sp'), may hold values from -0.59765625 to 0.59765625
- mixed_input: bfloat16 [3072, 2048], P('sp'), may hold values from -6 to 6
- route_ids: int32 [3072, 2], P('sp'), may hold values from 0 to 15, all different within a row; in each aligned block of 192 rows (0 to 191, 192 to 383, ...) at most 48 rows name the same one
- route_gates: float32 [3072, 2], P('sp'), may hold values from 0.25 to 1.5
- expert_gate: bfloat16 [16, 2048, 1024], P('sp', None, 'tp'), may hold values from -0.125 to 0.125
- expert_up: bfloat16 [16, 2048, 1024], P('sp', None, 'tp'), may hold values from -0.125 to 0.125
- expert_down: bfloat16 [16, 1024, 2048], P('sp', 'tp'), may hold values from -0.1875 to 0.1875
- projection: bfloat16 [2048, 1024], P(None, 'tp'), may hold values from -0.1875 to 0.1875
- mixer_output: bfloat16 [3072, 1024], P('sp', 'tp'), may hold values from -6 to 6
- query_rows: bfloat16 [3072, 512], P('sp', 'tp'), may hold values from -6 to 6
- key_rows: bfloat16 [3072, 512], P('sp', 'tp'), may hold values from -0.75 to 0.75
- value_rows: bfloat16 [3072, 1024], P('sp', 'tp'), may hold values from -6 to 6
- log_forward: float32 [3072, 512], P('sp', 'tp'), may hold values from -0.25 to 0, as said below
- log_backward: float32 [3072, 512], P('sp', 'tp'), may hold values from -0.25 to 0, as said below
Outputs:
- gate_grad: float32 [16, 2048, 1024], P('sp', None, 'tp')
- up_grad: float32 [16, 2048, 1024], P('sp', None, 'tp')
- down_grad: float32 [16, 1024, 2048], P('sp', 'tp')
- projection_grad: float32 [2048, 1024], P('sp', 'tp')
- query_grad: float32 [3072, 512], P('sp', 'tp')
- key_grad: float32 [3072, 512], P('sp', 'tp')
- value_grad: float32 [3072, 1024], P('sp', 'tp')
- log_forward_grad: float32 [3072, 512], P('sp', 'tp')
- log_backward_grad: float32 [3072, 512], P('sp', 'tp')
Inputs may be any that keep to these rules, and one draw needn't show every extreme that they name: `route_ids`: in the rows of one device no expert is named by more than 48 routes, a bound that some block reaches in the rows of some device; the 2 experts of a token differ. `log_forward`: strictly negative. `log_backward`: strictly negative.
All inputs are finite; a program needn't handle non-finite values.
Results may differ from a plain program's by a relative error of at most 0.006.
Values may be sent and summed in bfloat16 or wider, within the bound.
A program may use at most 192 MiB of HBM per device.

v0:
```python
import jax
import jax.numpy as jnp
from jax import lax
from jax.sharding import PartitionSpec as P

DK = 32
DV = 64
BLK = 64


topmost_precision = lax.Precision.HIGHEST


def entering_2(value, axis, join, neutral, backward):
    count, mine = (lax.axis_size(axis), lax.axis_index(axis))
    pieces = jax.tree.map(lambda part: lax.all_gather(part, axis), value)
    if backward:
        pieces = jax.tree.map(lambda part: part[::-1], pieces)
        mine = count - 1 - mine
    so_far = jax.tree.map(
        lambda part, zero: jnp.full_like(part, 0) + jnp.asarray(zero, part.dtype), value, neutral
    )

    def hop(position, so_far):
        longer = join(so_far, jax.tree.map(lambda part: part[position], pieces))
        return jax.tree.map(lambda new, old: jnp.where(position < mine, new, old), longer, so_far)

    return lax.fori_loop(0, count - 1, hop, so_far)


def decayed_pass(query_stack, key_matrix, value_matrix, log_rate, entering):
    count = query_stack.shape[0]
    head_count = query_stack.shape[1]
    key_width = query_stack.shape[2]
    value_width = value_matrix.shape[2]
    blocks = count // BLK
    query_blocks = query_stack.reshape(blocks, BLK, head_count, key_width)
    key_blocks = key_matrix.reshape(blocks, BLK, head_count, key_width)
    value_blocks = value_matrix.reshape(blocks, BLK, head_count, value_width)
    running_prefix = jnp.cumsum(log_rate.reshape(blocks, BLK, head_count, key_width), axis=1)
    last_cum = running_prefix[:, -1:]
    increment = jnp.einsum(
        "nlhk,nlhv->nhkv",
        key_blocks * jnp.exp(last_cum - running_prefix),
        value_blocks,
        precision=topmost_precision,
    )
    decay = jnp.exp(last_cum[:, 0])

    def advance(carried, inputs):
        factor, added = inputs
        return (factor[..., None] * carried + added, carried)

    final_state, entering_states = lax.scan(advance, entering, (decay, increment))
    inter_part = jnp.einsum(
        "nlhk,nhkv->nlhv",
        query_blocks * jnp.exp(running_prefix),
        entering_states,
        precision=topmost_precision,
    )
    middle = running_prefix[:, BLK // 2 - 1 : BLK // 2]
    scores = jnp.einsum(
        "nlhk,nmhk->nhlm",
        query_blocks * jnp.exp(running_prefix - middle),
        key_blocks * jnp.exp(middle - running_prefix),
        precision=topmost_precision,
    )
    lower_mask = jnp.tril(jnp.ones((BLK, BLK), bool))
    scores = jnp.where(lower_mask, scores, jnp.float32(0.0))
    intra_part = jnp.einsum("nhlm,nmhv->nlhv", scores, value_blocks, precision=topmost_precision)
    return ((inter_part + intra_part).reshape(count, head_count, value_width), final_state)


def reverse_rows(source_array):
    return jnp.flip(source_array, axis=0)


def span_summary(key_matrix, value_matrix, log_rate):
    running_prefix = jnp.cumsum(log_rate, axis=0)
    summed_values = running_prefix[-1]
    carried = jnp.einsum(
        "zly,zlq->lyq",
        key_matrix * jnp.exp(summed_values[None] - running_prefix),
        value_matrix,
        precision=topmost_precision,
    )
    return (jnp.exp(summed_values), carried, running_prefix)


def combine_maps(earlier, later):
    return tuple(
        (
            (
                earlier_pair[0] * later_pair[0],
                later_pair[0][..., None] * earlier_pair[1] + later_pair[1],
            )
            for earlier_pair, later_pair in zip(earlier, later)
        )
    )


def mixer_grads(query_rows, key_rows, value_rows, log_forward, log_backward, mix_grad):
    tok_count = query_rows.shape[0]
    head_count = query_rows.shape[1] // DK
    query_scaling = DK ** (-0.5)

    def by_heads(source_array, head_width):
        return source_array.astype(jnp.float32).reshape(tok_count, head_count, head_width)

    query_stack = by_heads(query_rows, DK)
    key_matrix = by_heads(key_rows, DK)
    value_matrix = by_heads(value_rows, DV)
    rate_fwd = by_heads(log_forward, DK)
    rate_bwd = by_heads(log_backward, DK)
    output_gradient = by_heads(mix_grad, DV)
    decay_fwd, carried_fwd, forward_running_total = span_summary(key_matrix, value_matrix, rate_fwd)
    decay_bwd, carried_bwd, cumul_bwd = span_summary(
        reverse_rows(key_matrix), reverse_rows(value_matrix), reverse_rows(rate_bwd)
    )
    pulled_fwd = jnp.einsum(
        "zly,zlq->lyq",
        query_stack * query_scaling * jnp.exp(forward_running_total),
        output_gradient,
        precision=topmost_precision,
    )
    pulled_bwd = jnp.einsum(
        "zly,zlq->lyq",
        reverse_rows(query_stack) * query_scaling * jnp.exp(cumul_bwd),
        reverse_rows(output_gradient),
        precision=topmost_precision,
    )
    unit_decay = jnp.ones_like(decay_fwd)
    empty_state = jnp.zeros_like(carried_fwd)
    identity_maps = ((unit_decay, empty_state), (unit_decay, empty_state))
    lower_maps = entering_2(
        ((decay_fwd, carried_fwd), (decay_bwd, pulled_bwd)),
        "sp",
        combine_maps,
        identity_maps,
        False,
    )
    upper_maps = entering_2(
        ((decay_bwd, carried_bwd), (decay_fwd, pulled_fwd)), "sp", combine_maps, identity_maps, True
    )
    state_fwd = lower_maps[0][1]
    leave_bwd_grad = lower_maps[1][1]
    state_bwd = upper_maps[0][1]
    leave_fwd_grad = upper_maps[1][1]

    def local_mixer(query_in, key_in, value_in, forward_in, backward_in):
        out_fwd, leave_fwd = decayed_pass(
            query_in * query_scaling, key_in, value_in, forward_in, state_fwd
        )
        out_bwd, leave_bwd = decayed_pass(
            reverse_rows(query_in) * query_scaling,
            reverse_rows(key_in),
            reverse_rows(value_in),
            reverse_rows(backward_in),
            state_bwd,
        )
        return (out_fwd + reverse_rows(out_bwd), leave_fwd, leave_bwd)

    _, pullback = jax.vjp(local_mixer, query_stack, key_matrix, value_matrix, rate_fwd, rate_bwd)
    grads = pullback((output_gradient, leave_fwd_grad, leave_bwd_grad))
    return tuple((gradient.reshape(tok_count, -1) for gradient in grads))


def local(
    cotangent,
    mixed_input,
    route_ids,
    route_gates,
    expert_gate,
    expert_up,
    expert_down,
    projection,
    mixer_output,
    query_rows,
    key_rows,
    value_rows,
    log_forward,
    log_backward,
):
    tok_count = cotangent.shape[0]
    feature_count = cotangent.shape[1]
    groups = lax.axis_size("sp")
    slot_count = 4 * tok_count // groups
    route_count = route_ids.shape[1]
    flat_ids = route_ids.reshape(-1)
    assigned = flat_ids.shape[0]
    onehot = (flat_ids[:, None] == jnp.arange(groups, dtype=jnp.int32)[None, :]).astype(jnp.int32)
    rank = jnp.sum((jnp.cumsum(onehot, axis=0) - 1) * onehot, axis=1)
    destination = flat_ids * slot_count + rank
    source = (
        jnp.full((groups * slot_count,), assigned, jnp.int32)
        .at[destination]
        .set(jnp.arange(assigned, dtype=jnp.int32))
    )
    token_of = source // route_count
    gate_padded = jnp.concatenate([route_gates.reshape(-1), jnp.zeros((1,), jnp.float32)])
    cot_padded = jnp.concatenate([cotangent, jnp.zeros((1, feature_count), jnp.bfloat16)], axis=0)
    input_padded = jnp.concatenate(
        [mixed_input, jnp.zeros((1, feature_count), jnp.bfloat16)], axis=0
    )
    routed_cot = (
        (gate_padded[source][:, None] * cot_padded[token_of].astype(jnp.float32))
        .astype(jnp.bfloat16)
        .reshape(groups, slot_count, feature_count)
    )
    routed_tok = input_padded[token_of].reshape(groups, slot_count, feature_count)
    w_gate = expert_gate[0]
    w_up = expert_up[0]
    w_down = expert_down[0]
    contract_last = (((1,), (1,)), ((), ()))
    contract_first = (((0,), (0,)), ((), ()))
    cot_in = lax.all_to_all(routed_cot, "sp", split_axis=0, concat_axis=0, tiled=True)
    tok_in = lax.all_to_all(routed_tok, "sp", split_axis=0, concat_axis=0, tiled=True)
    row_total = cot_in.shape[0] * cot_in.shape[1]
    cot_block = cot_in.reshape(row_total, feature_count)
    tok_block = tok_in.reshape(row_total, feature_count)
    gate_pre = jnp.dot(tok_block, w_gate, preferred_element_type=jnp.float32)
    up_pre = jnp.dot(tok_block, w_up, preferred_element_type=jnp.float32)
    sigmoid_gate = jax.nn.sigmoid(gate_pre)
    silu_gate = gate_pre * sigmoid_gate
    hidden = (silu_gate * up_pre).astype(jnp.bfloat16)
    hidden_grad = lax.dot_general(
        cot_block, w_down, contract_last, preferred_element_type=jnp.float32
    )
    slope = sigmoid_gate * (1.0 + gate_pre * (1.0 - sigmoid_gate))
    gate_pre_grad = (hidden_grad * up_pre * slope).astype(jnp.bfloat16)
    up_pre_grad = (hidden_grad * silu_gate).astype(jnp.bfloat16)
    partial_value = lax.dot_general(
        gate_pre_grad, w_gate, contract_last, preferred_element_type=jnp.float32
    )
    partial_value = partial_value + lax.dot_general(
        up_pre_grad, w_up, contract_last, preferred_element_type=jnp.float32
    )
    down_term = lax.dot_general(
        hidden, cot_block, contract_first, preferred_element_type=jnp.float32
    )
    gate_term = lax.dot_general(
        tok_block, gate_pre_grad, contract_first, preferred_element_type=jnp.float32
    )
    up_term = lax.dot_general(
        tok_block, up_pre_grad, contract_first, preferred_element_type=jnp.float32
    )
    summed = lax.psum_scatter(
        partial_value.astype(jnp.bfloat16), "tp", scatter_dimension=1, tiled=True
    )
    returned = lax.all_to_all(
        summed.reshape(cot_in.shape[0], cot_in.shape[1], summed.shape[1]),
        "sp",
        split_axis=0,
        concat_axis=0,
        tiled=True,
    )
    expert_terms = (gate_term, up_term, down_term)
    column_count = returned.shape[2]
    own_cot = lax.dynamic_slice_in_dim(
        cotangent, lax.axis_index("tp") * column_count, column_count, 1
    )
    per_route = returned.reshape(groups * slot_count, column_count)[destination].reshape(
        tok_count, route_count, column_count
    )
    mid_grad = (
        jnp.sum(per_route.astype(jnp.float32), axis=1) + own_cot.astype(jnp.float32)
    ).astype(jnp.bfloat16)
    mid_grad = lax.all_gather(mid_grad, "tp", axis=1, tiled=True)
    mix_grad = jnp.dot(mid_grad, projection, preferred_element_type=jnp.float32).astype(
        jnp.bfloat16
    )
    projection_grad = lax.psum_scatter(
        lax.dot_general(mid_grad, mixer_output, contract_first, preferred_element_type=jnp.float32),
        "sp",
        scatter_dimension=0,
        tiled=True,
    )
    query_grad, key_grad, value_grad, log_forward_grad, log_backward_grad = mixer_grads(
        query_rows, key_rows, value_rows, log_forward, log_backward, mix_grad
    )
    return (
        expert_terms[0][None],
        expert_terms[1][None],
        expert_terms[2][None],
        projection_grad,
        query_grad,
        key_grad,
        value_grad,
        log_forward_grad,
        log_backward_grad,
    )


def solution(mesh):
    return jax.shard_map(
        local,
        mesh=mesh,
        in_specs=(
            P("sp", None),
            P("sp", None),
            P("sp", None),
            P("sp", None),
            P("sp", None, "tp"),
            P("sp", None, "tp"),
            P("sp", "tp", None),
            P(None, "tp"),
            P("sp", "tp"),
            P("sp", "tp"),
            P("sp", "tp"),
            P("sp", "tp"),
            P("sp", "tp"),
            P("sp", "tp"),
        ),
        out_specs=(
            P("sp", None, "tp"),
            P("sp", None, "tp"),
            P("sp", "tp", None),
            P("sp", "tp"),
            P("sp", "tp"),
            P("sp", "tp"),
            P("sp", "tp"),
            P("sp", "tp"),
            P("sp", "tp"),
        ),
        check_vma=False,
    )
```

profile of v0, /device:TPU:0, one launch (start us, length us, event | category | flops | bytes accessed | tf_op | source)
XLA Modules:
  0.0 639.6 jit_solution(12209840836283323716)
XLA Ops:
  11.5 2.9 scatter_custom_fusion
  15.6 4.2 gather_fusion
  19.9 8.4 %all-to-all-start = ((bf16[16,48,2048]{2,1,0:T(8,128)(2,1)}), bf16[16,48,2048]{2,1,0:T(8,128)(2,1)}, u32[]{:S(2)}, u32[]{:S(2)}) async-start(bf16[16,48,2048]{2,1,0:T(8,128)(2,1)} %bitcast.314), calls=%async_computation | async-start | bytes 6291456 | tf_op jit(solution)/shard_map/all_to_all | solution.py:217
  29.5 4.2 gather_fusion.2
  34.0 5.0 gather_fusion.1
  39.1 4.1 fusion.6
  43.2 46.0 %all-to-all-done = bf16[16,48,2048]{2,1,0:T(8,128)(2,1)} async-done(((bf16[16,48,2048]{2,1,0:T(8,128)(2,1)}), bf16[16,48,2048]{2,1,0:T(8,128)(2,1)}, u32[]{:S(2)}, u32[]{:S(2)}) %all-to-all-start) | async-done | bytes 3145760 | tf_op jit(solution)/shard_map/all_to_all | solution.py:217
  89.2 15.2 %all-to-all-start.1 = ((bf16[16,48,2048]{2,1,0:T(8,128)(2,1)}), bf16[16,48,2048]{2,1,0:T(8,128)(2,1)}, u32[]{:S(2)}, u32[]{:S(2)}) async-start(bf16[16,48,2048]{2,1,0:T(8,128)(2,1)} %fusion.6), calls=%async_computation.1 | async-start | bytes 6291456 | tf_op jit(solution)/shard_map/all_to_all | solution.py:216
  104.7 5.5 fusion.12
  110.2 4.8 fusion.9
  115.0 50.0 %all-to-all-done.1 = bf16[16,48,2048]{2,1,0:T(8,128)(2,1)} async-done(((bf16[16,48,2048]{2,1,0:T(8,128)(2,1)}), bf16[16,48,2048]{2,1,0:T(8,128)(2,1)}, u32[]{:S(2)}, u32[]{:S(2)}) %all-to-all-start.1) | async-done | bytes 3145760 | tf_op jit(solution)/shard_map/all_to_all | solution.py:216
  165.1 5.7 multiply_convert_fusion.1
  173.0 3.5 add_convert_fusion
  178.1 18.0 %reduce-scatter.3.cloned.1.call-done = bf16[768,1024]{1,0:T(8,128)(2,1)} async-done(((bf16[768,2048]{1,0:T(8,128)(2,1)}), bf16[768,1024]{1,0:T(8,128)(2,1)}) %reduce-scatter.3.cloned.1.call-update) | async-done | bytes 1572880 | tf_op jit(solution)/shard_map/reduce_scatter | solution.py:247
  196.0 6.9 %all-to-all-start.2 = ((bf16[16,48,1024]{2,1,0:T(8,128)(2,1)}), bf16[16,48,1024]{2,1,0:T(8,128)(2,1)S(1)}, u32[]{:S(2)}, u32[]{:S(2)}) async-start(bf16[16,48,1024]{2,1,0:T(8,128)(2,1)} %bitcast.337), calls=%async_computation.3 | async-start | bytes 3145728 | tf_op jit(solution)/shard_map/all_to_all | solution.py:250
  203.6 18.0 %reduce-window.24 = f32[32,8,2,128]{3,1,2,0:T(8,128)S(1)} reduce-window(f32[32,8,2,128]{3,1,2,0:T(8,128)S(1)} %pad_bitcast_fusion.1, f32[]{:T(128)} %constant.233.clone.1), window={size=1x1x1x128 pad=0_0x0_0x0_0x127_0}, to_apply=%region_8.9 | reduce-window | flops 8323072 | bytes 524292 | tf_op jit(solution)/shard_map/reduce-window.2
  223.9 18.0 %reduce-window.26 = f32[32,8,2,128]{3,1,2,0:T(8,128)S(1)} reduce-window(f32[32,8,2,128]{3,1,2,0:T(8,128)S(1)} %pad_bitcast_fusion, f32[]{:T(128)} %constant.233.clone.1), window={size=1x1x1x128 pad=0_0x0_0x0_0x127_0}, to_apply=%region_10.11 | reduce-window | flops 8323072 | bytes 524292 | tf_op jit(solution)/shard_map/reduce-window.4
  249.2 3.8 exponential_multiply_fusion.3
  253.0 2.2 fusion.25
  255.3 2.7 gather_fusion.3
  258.0 2.1 reshape.294
  260.1 2.9 reduce_sum.114
  264.5 2.4 all_gather.39
  269.2 2.7 fusion.23
  287.9 41.6 %all_gather.40 = f32[16,8,32]{2,1,0:T(8,128)S(1)} all-gather(f32[1,8,32]{2,1,0:T(8,128)S(1)} %copy-done.59), channel_id=1, replica_groups=mesh['sp'=16,'tp'=2] {'sp'}, dimensions={0}, use_global_device_ids=true | all-gather | bytes 17408 | tf_op jit(solution)/shard_map/all_gather | solution.py:16
  330.2 36.2 %all_gather.43 = f32[16,8,32]{2,1,0:T(8,128)S(1)} all-gather(f32[1,8,32]{2,1,0:T(8,128)S(1)} %get-tuple-element.888), channel_id=1, replica_groups=mesh['sp'=16,'tp'=2] {'sp'}, dimensions={0}, use_global_device_ids=true | all-gather | bytes 17408 | tf_op jit(solution)/shard_map/all_gather | solution.py:16
  372.6 2.5 fusion.28
  375.1 2.5 convolution_select_fusion.1
  378.9 2.5 convolution_select_fusion
  381.4 3.3 rev.55
  384.7 5.8 convolution_bitcast_fusion.1
  390.5 5.9 convolution_bitcast_fusion.2
  396.4 5.9 convolution_bitcast_fusion
  406.6 2.2 copy.305
  410.3 2.0 copy.338
  412.3 3.5 fusion.19
  415.8 2.4 convolution_select_fusion.2
  418.1 2.1 fusion.38
  420.3 2.7 fusion.32
  423.1 2.4 fusion.35
  427.8 2.2 convolution_bitcast_fusion.10
  430.0 2.1 convolution_bitcast_fusion.8
  434.0 2.7 fusion.93
  436.7 3.1 rev.57
  439.9 38.7 %while.100 = (s32[]{:T(128)}, f32[8,32,64]{2,1,0:T(8,128)S(1)}, f32[8,32,64]{2,1,0:T(8,128)S(1)}, s32[]{:T(128)}, f32[16,8,32]{2,1,0:T(8,128)}, /*index=5*/f32[1...) while((s32[]{:T(128)}, f32[8,32,64]{2,1,0:T(8,128)S(1)}, ...), condition=%wide.region_13.14_spmd.clone, body=%wide.region_12.13_spmd.clone.sunk | while | flops 131076 | bytes 399493 | solution.py:28
  479.4 5.2 while.96
  484.6 19.9 %all-gather.15.cloned.1.call-done = f32[128,32,64]{2,1,0:T(8,128)} async-done(((f32[8,32,64]{2,1,0:T(8,128)}), f32[128,32,64]{2,1,0:T(8,128)}) %all-gather.15.cloned.1.call-update) | async-done | bytes 1048592 | tf_op jit(solution)/shard_map/all_gather | solution.py:16
  504.5 38.2 %while.101 = (s32[]{:T(128)}, f32[8,32,64]{2,1,0:T(8,128)S(1)}, f32[8,32,64]{2,1,0:T(8,128)S(1)}, s32[]{:T(128)}, f32[16,8,32]{2,1,0:T(8,128)}, /*index=5*/f32[1...) while((s32[]{:T(128)}, f32[8,32,64]{2,1,0:T(8,128)S(1)}, ...), condition=%wide.region_18.19_spmd.clone, body=%wide.region_17.18_spmd.clone.sunk | while | flops 131076 | bytes 399493 | solution.py:28
  543.5 5.5 while.98
  549.0 3.7 fusion.18
  552.7 2.3 copy.368
  555.8 5.2 while.97
  561.8 5.5 while.99
  567.4 3.7 fusion.17
  571.1 2.3 copy.369
  573.4 2.4 bitcast_add_fusion.8
  575.8 2.3 copy.370
  580.0 2.7 convolution_bitcast_fusion.5
  582.7 2.8 fusion.62
  588.2 3.5 pad_add_fusion
  595.4 2.9 fusion.73
  600.3 2.8 pad_add_fusion.1
  605.0 19.4 %fusion.92 = f32[3,64,8,32]{3,2,1,0:T(8,128)S(1)} fusion(f32[3,64,8,32]{3,2,1,0:T(8,128)S(1)} %copy.385), kind=kOutput, calls=%fused_computation.198 | output fusion | flops 3096576 | bytes 393216 | tf_op jit(solution)/shard_map/transpose(jvp(jit(cumsum)))/reduce_window_sum | solution.py:40
  629.8 2.0 reshape.343
  (411 shorter events, 175.6 us)
Async XLA Ops:
  8.0 102.2 %copy-start = (bf16[1,2048,512]{2,1,0:T(8,128)(2,1)S(1)}, bf16[1,2048,512]{2,1,0:T(8,128)(2,1)}, u32[]{:S(2)}) copy-start(bf16[1,2048,512]{2,1,0:T(8,128)(2,1)} %param.30) | copy-start | bytes 6291460
  19.9 69.3 %all-to-all-start = ((bf16[16,48,2048]{2,1,0:T(8,128)(2,1)}), bf16[16,48,2048]{2,1,0:T(8,128)(2,1)}, u32[]{:S(2)}, u32[]{:S(2)}) async-start(bf16[16,48,2048]{2,1,0:T(8,128)(2,1)} %bitcast.314), calls=%async_computation | async-start | bytes 6291456 | tf_op jit(solution)/shard_map/all_to_all | solution.py:217
  29.5 4.2 copy-start.60
  89.2 75.9 %all-to-all-start.1 = ((bf16[16,48,2048]{2,1,0:T(8,128)(2,1)}), bf16[16,48,2048]{2,1,0:T(8,128)(2,1)}, u32[]{:S(2)}, u32[]{:S(2)}) async-start(bf16[16,48,2048]{2,1,0:T(8,128)(2,1)} %fusion.6), calls=%async_computation.1 | async-start | bytes 6291456 | tf_op jit(solution)/shard_map/all_to_all | solution.py:216
  104.4 91.7 %reduce-scatter.3.cloned.1.call-start = ((), (), s32[]{:S(2)}) async-start(), calls=%async_computation.5 | async-start | bytes 4718592 | tf_op jit(solution)/shard_map/reduce_scatter | solution.py:247
  170.8 2.2 copy-start.29
  177.8 18.3 %copy-start.27 = (f32[256,8,32]{0,2,1:T(8,128)}, f32[256,8,32]{0,2,1:T(8,128)S(1)}, u32[]{:S(2)}) copy-start(f32[256,8,32]{0,2,1:T(8,128)S(1)} %reverse.5) | copy-start | bytes 786436
  196.0 59.2 %all-to-all-start.2 = ((bf16[16,48,1024]{2,1,0:T(8,128)(2,1)}), bf16[16,48,1024]{2,1,0:T(8,128)(2,1)S(1)}, u32[]{:S(2)}, u32[]{:S(2)}) async-start(bf16[16,48,1024]{2,1,0:T(8,128)(2,1)} %bitcast.337), calls=%async_computation.3 | async-start | bytes 3145728 | tf_op jit(solution)/shard_map/all_to_all | solution.py:250
  203.0 20.6 %copy-start.43 = (f32[192,256]{1,0:T(8,128)S(1)}, f32[192,256]{1,0:T(8,128)}, u32[]{:S(2)}) copy-start(f32[192,256]{1,0:T(8,128)} %param.38) | copy-start | bytes 589828
  203.0 178.5 %all-gather.9.cloned.1.call-start = ((), (), s32[]{:S(2)}) async-start(), calls=%async_computation.7 | async-start | bytes 2228224 | tf_op jit(solution)/shard_map/all_gather | solution.py:16
  223.7 20.2 %copy-start.55 = (bf16[192,256]{1,0:T(8,128)(2,1)S(1)}, bf16[192,256]{1,0:T(8,128)(2,1)}, u32[]{:S(2)}) copy-start(bf16[192,256]{1,0:T(8,128)(2,1)} %param.36) | copy-start | bytes 294916
  241.9 2.5 copy-start.56
  242.5 3.1 copy-start.42
  244.0 2.6 copy-start.34
  255.2 181.5 %all-gather.11.cloned.1.call-start = ((), (), s32[]{:S(2)}) async-start(), calls=%async_computation.8 | async-start | bytes 2228224 | tf_op jit(solution)/shard_map/all_gather | solution.py:16
  263.0 3.9 copy-start.28
  266.9 5.0 copy-start.6
  266.9 5.1 copy-start.24
  269.2 4.3 copy-start.25
  271.9 212.7 %all-gather.13.cloned.1.call-start = ((), (), s32[]{:S(2)}) async-start(), calls=%async_computation.9 | async-start | bytes 2228224 | tf_op jit(solution)/shard_map/all_gather | solution.py:16
  273.4 231.1 %all-gather.15.cloned.1.call-start = ((), (), s32[]{:S(2)}) async-start(), calls=%async_computation.10 | async-start | bytes 2228224 | tf_op jit(solution)/shard_map/all_gather | solution.py:16
  277.0 5.3 copy-start.21
  279.0 5.4 copy-start.35
  282.3 4.9 copy-start.37
  282.3 5.7 copy-start.59
  283.5 83.6 %copy-start.20 = (f32[3,64,8,32]{3,2,1,0:T(8,128)}, f32[3,64,8,32]{3,2,1,0:T(8,128)S(1)}, u32[]{:S(2)}) copy-start(f32[3,64,8,32]{3,2,1,0:T(8,128)S(1)} %fusion.90) | copy-start | bytes 589828
  329.6 37.5 %copy-start.45 = (f32[16,8,32]{2,1,0:T(8,128)}, f32[16,8,32]{2,1,0:T(8,128)S(1)}, u32[]{:S(2)}) copy-start(f32[16,8,32]{2,1,0:T(8,128)S(1)} %all_gather.40) | copy-start | bytes 49156
  368.9 8.7 %copy-start.2 = (f32[192,8,64]{2,1,0:T(8,128)}, f32[192,8,64]{2,1,0:T(8,128)S(1)}, u32[]{:S(2)}) copy-start(f32[192,8,64]{2,1,0:T(8,128)S(1)} %copy.307) | copy-start | bytes 1179652
  368.9 6.2 copy-start.44
  368.9 6.2 copy-start.52
  372.6 5.0 copy-start.12
  372.6 5.0 copy-start.47
  375.0 3.9 copy-start.4
  381.4 3.3 copy-start.41
  384.7 5.8 copy-start.39
  390.5 5.9 copy-start.61
  390.5 5.9 copy-start.62
  396.4 5.9 copy-start.26
  396.4 6.8 %copy-start.30 = (bf16[192,512]{1,0:T(8,128)(2,1)S(1)}, bf16[192,512]{1,0:T(8,128)(2,1)}, u32[]{:S(2)}) copy-start(bf16[192,512]{1,0:T(8,128)(2,1)} %convolution_convert_fusion) | copy-start | bytes 589828
  405.6 3.2 copy-start.16
  420.2 211.6 %reduce-scatter.5.cloned.1.call-start = ((), (), s32[]{:S(2)}) async-start(), calls=%async_computation.6 | async-start | bytes 4456448 | tf_op jit(solution)/shard_map/reduce_scatter | solution.py:272
  420.3 2.8 copy-start.23
  420.3 5.2 copy-start.3
  425.5 4.5 copy-start.8
  427.8 4.3 copy-start.22
  430.0 4.0 copy-start.7
  430.0 4.0 copy-start.53
  439.9 39.5 %copy-start.51 = (f32[3,8,32]{2,1,0:T(8,128)S(1)}, f32[3,8,32]{2,1,0:T(8,128)}, u32[]{:S(2)}) copy-start(f32[3,8,32]{2,1,0:T(8,128)} %fusion.85) | copy-start | bytes 9220
  543.5 5.5 copy-start.49
  549.0 6.8 %copy-start.50 = (f32[3,8,32]{2,1,0:T(8,128)S(1)}, f32[3,8,32]{2,1,0:T(8,128)}, u32[]{:S(2)}) copy-start(f32[3,8,32]{2,1,0:T(8,128)} %fusion.86) | copy-start | bytes 9220
  567.4 6.0 copy-start.57
  580.0 2.7 copy-start.11
  582.7 2.8 copy-start.19
  591.7 2.9 copy-start.13
  591.7 2.9 copy-start.18
  591.7 3.7 copy-start.5
  591.7 3.7 copy-start.9
  595.4 3.0 copy-start.17
  595.4 3.2 copy-start.58
  595.4 4.9 copy-start.14
  595.4 4.9 copy-start.15
  595.4 4.9 copy-start.48
  605.0 20.9 %copy-start.32 = (f32[3,64,8,32]{1,3,2,0:T(8,128)S(1)}, f32[3,64,8,32]{1,3,2,0:T(8,128)}, u32[]{:S(2)}) copy-start(f32[3,64,8,32]{1,3,2,0:T(8,128)} %get-tuple-element.877) | copy-start | bytes 589828
  627.0 4.9 copy-start.1
  (8 other events, 11.1 us)
Sparse Core Ops, SparseCore 0:
  176.6 19.4 reduce-scatter.2
Sparse Core Ops, SparseCore 1:
  255.3 62.0 all-gather.8
  320.6 59.3 all-gather.10
  382.6 59.2 all-gather.12
  445.3 59.2 all-gather.14
  507.4 94.2 reduce-scatter.4
where the time goes:
time: 649 us; the launch traced here: 640 us
  local copies, waits for them, and re-layouts  145 us (22%)
  waiting for transfers between devices  134 us (21%)
  other arithmetic  129 us (20%)
  matrix products  102 us (16%)
  blocking collectives  80.2 us (12%)
  starting transfers between devices  31.5 us (5%)
  between operations  16.9 us (3%)
    all_gather x2, blocking collectives, entering_2(): pieces = jax.tree.map(lambda part: lax.all_gather(part, axis), value)  77.9 us
    all_to_all x1, waiting for transfers between devices, local(): lax.all_to_all(routed_cot, 'sp', split_axis=0, concat_axis=0, tiled=True)  50 us
    all_to_all x1, waiting for transfers between devices, local(): lax.all_to_all(routed_tok, 'sp', split_axis=0, concat_axis=0, tiled=True)  46 us
    mul x60, local copies, waits for them, and re-layouts, combine_maps(): later_pair[0][..., None] * earlier_pair[1] + later_pair[1]  41 us
    another operation x8, other arithmetic  37.3 us
    select_n x30, other arithmetic, hop(): jnp.where(position < mine, new, old)  34.8 us
    another operation x4, other arithmetic, decayed_pass(): jnp.cumsum(log_rate.reshape(blocks, BLK, head_count, key_width), axis=1)  23.5 us
    all_gather x4, waiting for transfers between devices, entering_2(): pieces = jax.tree.map(lambda part: lax.all_gather(part, axis), value)  20 us
  transfers between devices with their start and end apart: 9, of which 4 were waited for; matrix products, arithmetic and copies ran while one was open for 55% of the time, Pallas kernels for 0%

commit v1 on v0

v1 whole, which is shorter than its diff:
```python
import functools

import jax
import jax.numpy as jnp
from jax import lax
from jax.experimental import pallas as pl
from jax.experimental.pallas import tpu as pltpu
from jax.sharding import PartitionSpec as P

DK = 32
DV = 64
F32 = jnp.float32
BF16 = jnp.bfloat16
MESH = pl.DeviceIdType.MESH
HIGHEST = lax.Precision.HIGHEST
VMEM = pl.BlockSpec(memory_space=pltpu.VMEM)
ANY = pl.BlockSpec(memory_space=pl.ANY)
VMEM_LIMIT = 60 * 1024 * 1024


def dot(a, b, dims=((1,), (0,)), precision=None):
    return lax.dot_general(a, b, (dims, ((), ())), preferred_element_type=F32, precision=precision)


def triangle(count, lower):
    rows = lax.broadcasted_iota(jnp.int32, (count, count), 0)
    cols = lax.broadcasted_iota(jnp.int32, (count, count), 1)
    return rows >= cols if lower else rows <= cols


def head_lanes(head, width, total):
    lane = lax.broadcasted_iota(jnp.int32, (1, total), 1)
    return (lane >= head * width) & (lane < (head + 1) * width)


def block_states(wide, narrow, heads):
    full = dot(wide, narrow, ((0,), (0,)))
    keys = narrow.shape[1]
    total = jnp.zeros((DV, keys), F32)
    for head in range(heads):
        total = jnp.where(head_lanes(head, DK, keys), full[head * DV : (head + 1) * DV], total)
    return total


def prep_kernel(heads, k_ref, v_ref, lf_ref, lb_ref, cf_ref, cb_ref, tot_ref, st_ref, sb_ref):
    count, keys = k_ref.shape
    lower = triangle(count, True).astype(F32)
    upper = triangle(count, False).astype(F32)
    cf = dot(lower, lf_ref[...], precision=HIGHEST)
    cb = dot(upper, lb_ref[...], precision=HIGHEST)
    cf_ref[...] = cf
    cb_ref[...] = cb
    tf = cf[count - 1 : count]
    tb = cb[0:1]
    tot_ref[:, :keys] = jnp.broadcast_to(tf, (8, keys))
    tot_ref[:, keys:] = jnp.broadcast_to(tb, (8, keys))
    k = k_ref[...].astype(F32)
    v = v_ref[...]
    for slot, (total, running) in enumerate(((tf, cf), (tb, cb))):
        state = block_states(v, (k * jnp.exp(total - running)).astype(BF16), heads)
        st_ref[slot] = state
        sb_ref[slot] = state.astype(BF16)


def pull_kernel(heads, q_ref, do_ref, cf_ref, cb_ref, pulled_ref):
    q = q_ref[...].astype(F32) * (DK**-0.5)
    do = do_ref[...]
    for slot, ref in ((0, cb_ref), (1, cf_ref)):
        pulled_ref[slot] = block_states(do, (q * jnp.exp(ref[...])).astype(BF16), heads).astype(BF16)


def send_all(count, me, make):
    barrier = pltpu.get_barrier_semaphore()
    for step in range(1, count):
        pl.semaphore_signal(
            barrier, inc=1, device_id={"sp": lax.rem(me + step, count)}, device_id_type=MESH
        )
    pl.semaphore_wait(barrier, count - 1)
    copies = []
    for step in range(1, count):
        for copy in make(step, lax.rem(me + step, count), (me + step) // count):
            copy.start()
            copies.append(copy)
    for copy in copies:
        copy.wait()


def chain(count, me, slots, totals, low_cols, high_cols, out_ref):
    shape = out_ref.shape[1:]
    low = jnp.zeros(shape, F32)
    high = jnp.zeros(shape, F32)
    for step in range(count - 1, 0, -1):
        use = (me >= step).astype(F32)
        decay = jnp.exp(totals[step, 0:1, low_cols])
        low = (1.0 - use + use * decay) * low + use * slots[step].astype(F32)
    for step in range(1, count):
        use = (me < step).astype(F32)
        decay = jnp.exp(totals[step, 0:1, high_cols])
        high = (1.0 - use + use * decay) * high + use * slots[step].astype(F32)
    out_ref[0] = low
    out_ref[1] = high


def first_exchange(count, x_ref, tot_ref, out_ref, totals_ref, slots, got, send, recv, tsend, trecv):
    me = lax.axis_index("sp")
    keys = x_ref.shape[2]

    def make(step, target, half):
        return (
            pltpu.make_async_remote_copy(
                src_ref=x_ref.at[half], dst_ref=slots.at[step], send_sem=send.at[step],
                recv_sem=recv.at[step], device_id={"sp": target}, device_id_type=MESH,
            ),
            pltpu.make_async_remote_copy(
                src_ref=tot_ref, dst_ref=got.at[step], send_sem=tsend.at[step],
                recv_sem=trecv.at[step], device_id={"sp": target}, device_id_type=MESH,
            ),
        )

    send_all(count, me, make)
    totals_ref[0] = tot_ref[...]
    for step in range(1, count):
        totals_ref[step] = got[step]
    chain(count, me, slots, got, slice(0, keys), slice(keys, 2 * keys), out_ref)


def second_exchange(count, x_ref, totals_ref, out_ref, slots, send, recv):
    me = lax.axis_index("sp")
    keys = x_ref.shape[2]

    def make(step, target, half):
        return (
            pltpu.make_async_remote_copy(
                src_ref=x_ref.at[half], dst_ref=slots.at[step], send_sem=send.at[step],
                recv_sem=recv.at[step], device_id={"sp": target}, device_id_type=MESH,
            ),
        )

    send_all(count, me, make)
    chain(count, me, slots, totals_ref, slice(keys, 2 * keys), slice(0, keys), out_ref)


def grads_kernel(
    heads, q_ref, k_ref, v_ref, do_ref, cf_ref, cb_ref, st_ref, into_ref, leave_ref,
    dq_ref, dk_ref, dv_ref, df_ref, db_ref,
):
    count, keys = k_ref.shape
    scale = DK**-0.5
    q = q_ref[...].astype(F32) * scale
    k = k_ref[...].astype(F32)
    v = v_ref[...]
    do = do_ref[...]
    lower = triangle(count, True)
    upper = triangle(count, False)
    sides = []
    dv = None
    for side in range(2):
        running = (cf_ref, cb_ref)[side][...]
        total = running[count - 1 : count] if side == 0 else running[0:1]
        up = jnp.exp(running - 0.5 * total)
        down = jnp.exp(0.5 * total - running)
        entering = into_ref[side]
        leaving = leave_ref[1 - side]
        spread_in = jnp.concatenate(
            [jnp.where(head_lanes(h, DK, keys), entering, 0.0) for h in range(heads)], axis=0
        ).astype(BF16)
        spread_out = jnp.concatenate(
            [jnp.where(head_lanes(h, DK, keys), leaving, 0.0) for h in range(heads)], axis=0
        ).astype(BF16)
        tail = jnp.exp(total - running)
        dq = jnp.exp(running) * dot(do, spread_in)
        dk = tail * dot(v, spread_out)
        part = dot((k * tail).astype(BF16), spread_out, ((1,), (1,)))
        dv = part if dv is None else dv + part
        edge = jnp.sum((jnp.exp(total) * entering + st_ref[side]) * leaving, axis=0, keepdims=True)
        sides.append([(q * up).astype(BF16), (k * down).astype(BF16), up, down, dq, dk, edge])
    dv_ref[...] = dv
    inner = [[jnp.zeros((count, keys), F32) for _ in range(2)] for _ in range(2)]
    for head in range(heads):
        pair = slice(head // 2 * 2 * DV, (head // 2 * 2 + 2) * DV)
        half = head_lanes(head % 2, DV, 2 * DV)
        mask = head_lanes(head, DK, keys)
        do_pair = jnp.where(half, do[:, pair], jnp.zeros((), BF16))
        v_pair = v[:, pair]
        weights = dot(do_pair, v_pair, ((1,), (1,)))
        turned = dot(v_pair, do_pair, ((1,), (1,)))
        mixed = None
        for side in range(2):
            q_side, k_side = sides[side][:2]
            q_head = jnp.where(mask, q_side, jnp.zeros((), BF16))
            k_head = jnp.where(mask, k_side, jnp.zeros((), BF16))
            kept, kept_turned = (lower, upper) if side == 0 else (upper, lower)
            scores = jnp.where(kept_turned, dot(k_head, q_side, ((1,), (1,))), 0.0)
            mixed = scores if mixed is None else mixed + scores
            inner[side][0] += dot(jnp.where(kept, weights, 0.0).astype(BF16), k_head)
            inner[side][1] += dot(jnp.where(kept_turned, turned, 0.0).astype(BF16), q_head)
        dv_ref[:, pair] += dot(mixed.astype(BF16), do_pair)
    total_q = None
    for side in range(2):
        up, down, dq, dk, edge = sides[side][2:]
        dq = dq + up * inner[side][0]
        dk = dk + down * inner[side][1]
        gap = q * dq - k * dk
        sums = (upper if side == 0 else lower).astype(F32)
        (df_ref, db_ref)[side][...] = dot(sums, gap, precision=HIGHEST) + edge
        if side == 0:
            total_q, total_k = dq, dk
        else:
            dq_ref[...] = (total_q + dq) * scale
            dk_ref[...] = total_k + dk


def cost(flops, moved):
    return pl.CostEstimate(flops=flops, bytes_accessed=moved, transcendentals=0)


def params(identity=None):
    if identity is None:
        return pltpu.CompilerParams(vmem_limit_bytes=VMEM_LIMIT)
    return pltpu.CompilerParams(
        collective_id=identity, has_side_effects=True, vmem_limit_bytes=VMEM_LIMIT
    )


def shaped(shape, kind=F32):
    return jax.ShapeDtypeStruct(shape, kind)


def mixer_start(key_rows, value_rows, log_forward, log_backward):
    count, keys = key_rows.shape
    heads = keys // DK
    groups = lax.axis_size("sp")
    cf, cb, total, state, state_sent = pl.pallas_call(
        functools.partial(prep_kernel, heads),
        out_shape=(
            shaped((count, keys)), shaped((count, keys)), shaped((8, 2 * keys)),
            shaped((2, DV, keys)), shaped((2, DV, keys), BF16),
        ),
        in_specs=[VMEM] * 4,
        out_specs=(VMEM,) * 5,
        compiler_params=params(),
        cost_estimate=cost(2 * 10**9, 2 * 10**6),
        name="mixer_prep",
    )(key_rows, value_rows, log_forward, log_backward)
    into, totals = pl.pallas_call(
        functools.partial(first_exchange, groups),
        out_shape=(shaped((2, DV, keys)), shaped((groups, 8, 2 * keys))),
        in_specs=[VMEM] * 2,
        out_specs=(VMEM,) * 2,
        scratch_shapes=[
            pltpu.VMEM((groups, DV, keys), BF16), pltpu.VMEM((groups, 8, 2 * keys), F32),
        ] + [pltpu.SemaphoreType.DMA((groups,))] * 4,
        compiler_params=params(1),
        cost_estimate=cost(10**6, 8 * 10**6),
        name="first_exchange",
    )(state_sent, total)
    return cf, cb, state, into, totals


def mixer_grads(query_rows, key_rows, value_rows, mix_grad, started):
    cf, cb, state, into, totals = started
    count, keys = key_rows.shape
    heads = keys // DK
    groups = lax.axis_size("sp")
    pulled = pl.pallas_call(
        functools.partial(pull_kernel, heads),
        out_shape=shaped((2, DV, keys), BF16),
        in_specs=[VMEM] * 4,
        out_specs=VMEM,
        compiler_params=params(),
        cost_estimate=cost(10**9, 10**6),
        name="mixer_pull",
    )(query_rows, mix_grad, cf, cb)
    leave = pl.pallas_call(
        functools.partial(second_exchange, groups),
        out_shape=shaped((2, DV, keys)),
        in_specs=[VMEM] * 2,
        out_specs=VMEM,
        scratch_shapes=[pltpu.VMEM((groups, DV, keys), BF16)]
        + [pltpu.SemaphoreType.DMA((groups,))] * 2,
        compiler_params=params(2),
        cost_estimate=cost(10**6, 8 * 10**6),
        name="second_exchange",
    )(pulled, totals)
    wide = value_rows.shape[1]
    return pl.pallas_call(
        functools.partial(grads_kernel, heads),
        out_shape=tuple(shaped((count, w)) for w in (keys, keys, wide, keys, keys)),
        in_specs=[VMEM] * 9,
        out_specs=(VMEM,) * 5,
        compiler_params=params(),
        cost_estimate=cost(8 * 10**9, 4 * 10**6),
        name="mixer_grads",
    )(query_rows, key_rows, value_rows, mix_grad, cf, cb, state, into, leave)


def dispatch_kernel(
    count, cot_ref, tok_ref, cot_out, tok_out, send, recv, relay_send, relay_recv, own_sem
):
    me = lax.axis_index("sp")
    core = lax.axis_index("tp")
    partner = 1 - core
    width = cot_ref.shape[2]
    columns = pl.ds(pl.multiple_of(core * width, width), width)
    pairs = ((cot_ref, cot_out), (tok_ref, tok_out))
    barrier = pltpu.get_barrier_semaphore()
    for step in range(1, count):
        pl.semaphore_signal(
            barrier, inc=1, device_id={"sp": lax.rem(me + step, count)}, device_id_type=MESH
        )
    pl.semaphore_signal(barrier, inc=1, device_id={"tp": partner}, device_id_type=MESH)
    pl.semaphore_wait(barrier, count)
    sent = []
    for step in range(1, count):
        target = lax.rem(me + step, count)
        for which, (source, result) in enumerate(pairs):
            copy = pltpu.make_async_remote_copy(
                src_ref=source.at[target],
                dst_ref=result.at[me, :, columns],
                send_sem=send.at[which, step],
                recv_sem=recv.at[which, step],
                device_id={"sp": target},
                device_id_type=MESH,
            )
            copy.start()
            sent.append(copy)
    relayed = []
    for which, (source, result) in enumerate(pairs):
        copy = pltpu.make_async_remote_copy(
            src_ref=source.at[me],
            dst_ref=result.at[me, :, columns],
            send_sem=relay_send.at[which, 0],
            recv_sem=relay_recv.at[which, 0],
            device_id={"tp": partner},
            device_id_type=MESH,
        )
        copy.start()
        relayed.append(copy)
    own = [
        pltpu.make_async_copy(source.at[me], result.at[me, :, columns], own_sem.at[which])
        for which, (source, result) in enumerate(pairs)
    ]
    for copy in own:
        copy.start()
    for step in range(1, count):
        origin = lax.rem(me + count - step, count)
        for which, (source, result) in enumerate(pairs):
            landed = result.at[origin, :, columns]
            pltpu.make_async_remote_copy(
                src_ref=source.at[origin],
                dst_ref=landed,
                send_sem=send.at[which, step],
                recv_sem=recv.at[which, step],
                device_id={"sp": origin},
                device_id_type=MESH,
            ).wait_recv()
            copy = pltpu.make_async_remote_copy(
                src_ref=landed,
                dst_ref=landed,
                send_sem=relay_send.at[which, step],
                recv_sem=relay_recv.at[which, step],
                device_id={"tp": partner},
                device_id_type=MESH,
            )
            copy.start()
            relayed.append(copy)
    for copy in sent:
        copy.wait_send()
    for copy in own:
        copy.wait()
    other = pl.ds(pl.multiple_of(partner * width, width), width)
    for copy in relayed:
        copy.wait_send()
    for step in range(count):
        origin = lax.rem(me + count - step, count)
        for which, (source, result) in enumerate(pairs):
            arrived = result.at[origin, :, other]
            pltpu.make_async_remote_copy(
                src_ref=arrived,
                dst_ref=arrived,
                send_sem=relay_send.at[which, step],
                recv_sem=relay_recv.at[which, step],
                device_id={"tp": partner},
                device_id_type=MESH,
            ).wait_recv()


def dispatch(routed_cot, routed_tok):
    groups, slots, width = routed_cot.shape
    whole = shaped((groups, slots, 2 * width), BF16)
    return pl.pallas_call(
        functools.partial(dispatch_kernel, groups),
        out_shape=(whole, whole),
        in_specs=[ANY] * 2,
        out_specs=(ANY,) * 2,
        scratch_shapes=[pltpu.SemaphoreType.DMA((2, groups))] * 4
        + [pltpu.SemaphoreType.DMA((2,))],
        compiler_params=pltpu.CompilerParams(collective_id=3, has_side_effects=True),
        cost_estimate=cost(10**6, 10**8),
        name="dispatch",
    )(routed_cot, routed_tok)


def local(
    cotangent,
    mixed_input,
    route_ids,
    route_gates,
    expert_gate,
    expert_up,
    expert_down,
    projection,
    mixer_output,
    query_rows,
    key_rows,
    value_rows,
    log_forward,
    log_backward,
):
    tok_count = cotangent.shape[0]
    feature_count = cotangent.shape[1]
    groups = lax.axis_size("sp")
    core = lax.axis_index("tp")
    half = feature_count // 2
    slot_count = 4 * tok_count // groups
    row_total = groups * slot_count
    contract_last = ((1,), (1,))
    contract_first = ((0,), (0,))
    swap = [(0, 1), (1, 0)]

    experts = jnp.arange(groups, dtype=jnp.int32)
    chosen = [(route_ids[:, place : place + 1] == experts[None, :]) for place in range(2)]
    named = (chosen[0] | chosen[1]).astype(BF16)
    steps = jnp.arange(tok_count, dtype=jnp.int32)
    before = dot((steps[:, None] > steps[None, :]).astype(BF16), named)
    place_of = before + (experts * slot_count).astype(F32)[None, :]
    rows = jnp.arange(row_total, dtype=jnp.int32)[:, None]
    hits = []
    for place in range(2):
        target = jnp.sum(jnp.where(chosen[place], place_of, 0.0), axis=1).astype(jnp.int32)
        hits.append(rows == target[None, :])
    pick = (hits[0] | hits[1]).astype(BF16)
    slot_gate = jnp.sum(
        jnp.where(hits[0], route_gates[:, 0][None, :], 0.0)
        + jnp.where(hits[1], route_gates[:, 1][None, :], 0.0),
        axis=1,
        keepdims=True,
    )
    own_cot = lax.dynamic_slice_in_dim(cotangent, core * half, half, 1)
    own_tok = lax.dynamic_slice_in_dim(mixed_input, core * half, half, 1)
    routed_cot = (slot_gate * dot(pick, own_cot)).astype(BF16)
    routed_tok = dot(pick, own_tok).astype(BF16)
    cot_in, tok_in = dispatch(
        routed_cot.reshape(groups, slot_count, half), routed_tok.reshape(groups, slot_count, half)
    )
    started = mixer_start(key_rows, value_rows, log_forward, log_backward)
    w_gate = expert_gate[0]
    w_up = expert_up[0]
    w_down = expert_down[0]
    cot_block = cot_in.reshape(row_total, feature_count)
    tok_block = tok_in.reshape(row_total, feature_count)
    gate_pre = dot(tok_block, w_gate)
    up_pre = dot(tok_block, w_up)
    sigmoid_gate = jax.nn.sigmoid(gate_pre)
    silu_gate = gate_pre * sigmoid_gate
    hidden = (silu_gate * up_pre).astype(BF16)
    hidden_grad = dot(cot_block, w_down, contract_last)
    slope = sigmoid_gate * (1.0 + gate_pre * (1.0 - sigmoid_gate))
    gate_pre_grad = (hidden_grad * up_pre * slope).astype(BF16)
    up_pre_grad = (hidden_grad * silu_gate).astype(BF16)
    partial_value = dot(gate_pre_grad, w_gate, contract_last)
    partial_value = (partial_value + dot(up_pre_grad, w_up, contract_last)).astype(BF16)
    mine = lax.dynamic_slice_in_dim(partial_value, core * half, half, 1)
    other = lax.dynamic_slice_in_dim(partial_value, (1 - core) * half, half, 1)
    came = lax.ppermute(other, "tp", swap)
    summed = (mine.astype(F32) + came.astype(F32)).astype(BF16)
    returned = lax.all_to_all(
        summed.reshape(groups, slot_count, half), "sp", split_axis=0, concat_axis=0, tiled=True
    ).reshape(row_total, half)
    down_term = dot(hidden, cot_block, contract_first)
    gate_term = dot(tok_block, gate_pre_grad, contract_first)
    up_term = dot(tok_block, up_pre_grad, contract_first)
    mid_half = (dot(pick, returned, contract_first) + own_cot.astype(F32)).astype(BF16)
    mid_other = lax.ppermute(mid_half, "tp", swap)
    first = core == 0
    mid_grad = jnp.concatenate(
        [jnp.where(first, mid_half, mid_other), jnp.where(first, mid_other, mid_half)], axis=1
    )
    mix_grad = dot(mid_grad, projection).astype(BF16)
    projection_grad = lax.psum_scatter(
        dot(mid_grad, mixer_output, contract_first), "sp", scatter_dimension=0, tiled=True
    )
    grads = mixer_grads(query_rows, key_rows, value_rows, mix_grad, started)
    return (gate_term[None], up_term[None], down_term[None], projection_grad, *grads)


def solution(mesh):
    rows = P("sp", None)
    both = P("sp", "tp")
    split_last = P("sp", None, "tp")
    split_first = P("sp", "tp", None)
    return jax.shard_map(
        local,
        mesh=mesh,
        in_specs=(
            rows, rows, rows, rows, split_last, split_last, split_first, P(None, "tp"),
            both, both, both, both, both, both,
        ),
        out_specs=(split_last, split_last, split_first, both, both, both, both, both, both),
        check_vma=False,
    )
```

time: 649 us -> 287 us (0.44); the launches traced: 640 us -> 287 us
  local copies, waits for them, and re-layouts: 145 us -> 5.28 us
  other arithmetic: 129 us -> 1.96 us
  Pallas kernels: 0 us -> 124 us
  waiting for transfers between devices: 134 us -> 38.1 us
  matrix products: 102 us -> 36.6 us
  starting transfers between devices: 31.5 us -> 0.18 us
  blocking collectives: 80.2 us -> 65.6 us
    pallas_call x0 -> x6, Pallas kernels: none -> 124 us  [the longest x1 64.4 us: dispatch(): pl.pallas_call(functools.partial(dispatch_kernel, groups), out_shape=(who...]
    all_to_all x3 -> x0, waiting for transfers between devices: 96 us -> none  [the longest x1 50 us: local(): lax.all_to_all(routed_cot, 'sp', split_axis=0, concat_axis=0, tiled=True)]
    all_gather x3 -> x0, blocking collectives: 80.2 us -> none  [the longest x2 77.9 us: entering_2(): pieces = jax.tree.map(lambda part: lax.all_gather(part, axis), value)]
    all_to_all x0 -> x1, blocking collectives: none -> 65.6 us  [local(): lax.all_to_all(summed.reshape(groups, slot_count, half), 'sp', split_axis...]
    dot_general x34 -> x14, matrix products: 102 us -> 36.6 us  [dot(): lax.dot_general(a, b, (dims, ((), ())), preferred_element_type=F32, preci...]
    another operation x12 -> x0, other arithmetic: 60.8 us -> none
    mul x77 -> x0, local copies, waits for them, and re-layouts: 43.7 us -> none  [the longest x60 41 us: combine_maps(): later_pair[0][..., None] * earlier_pair[1] + later_pair[1]]
    select_n x32 -> x1, other arithmetic: 34.8 us -> 1.05 us  [local(): jnp.where(first, mid_half, mid_other)]
  transfers between devices with their start and end apart: 9 -> 3, of which waited for: 4 -> 3; matrix products, arithmetic and copies ran while one was open for 55% -> 5% of each run, Pallas kernels for 0% -> 21%
where the time goes in v1:
time: 287 us
  Pallas kernels  124 us (43%)
  blocking collectives  65.6 us (23%)
  waiting for transfers between devices  38.1 us (13%)
  matrix products  36.6 us (13%)
  between operations  14.4 us (5%)
  local copies, waits for them, and re-layouts  5.28 us (2%)
    all_to_all x1, blocking collectives, local(): lax.all_to_all(summed.reshape(groups, slot_count, half), 'sp', split_axis...  65.6 us
    pallas_call x1, Pallas kernels, dispatch(): pl.pallas_call(functools.partial(dispatch_kernel, groups), out_shape=(who...  64.4 us
    dot_general x14, matrix products, dot(): lax.dot_general(a, b, (dims, ((), ())), preferred_element_type=F32, preci...  36.6 us
    reduce_scatter x1, waiting for transfers between devices, local(): lax.psum_scatter(dot(mid_grad, mixer_output, contract_first), 'sp', scatt...  32.8 us
    pallas_call x1, Pallas kernels, mixer_grads(): pl.pallas_call(functools.partial(second_exchange, groups), out_shape=shap...  24.8 us
    pallas_call x1, Pallas kernels, mixer_start(): pl.pallas_call(functools.partial(first_exchange, groups), out_shape=(shap...  24.7 us
  transfers between devices with their start and end apart: 3, of which 3 were waited for; matrix products, arithmetic and copies ran while one was open for 5% of the time, Pallas kernels for 21%

profile of v1, /device:TPU:0, one launch (start us, length us, event | category | flops | bytes accessed | tf_op | source)
XLA Modules:
  0.0 286.5 jit_solution(14893684845514171043)
XLA Ops:
  7.2 0.0 copy-start
  7.2 0.0 copy-start.13
  7.2 0.0 reduce-scatter.2.cloned.1.call-start
  7.3 0.9 fusion.35
  8.2 0.2 select_reduce_fusion.1
  8.4 0.8 fusion.34
  9.1 0.2 add_reduce_fusion
  9.3 2.9 %convolution_convert_fusion = bf16[768,1024]{1,0:T(8,128)(2,1)} fusion(bf16[192,2048]{1,0:T(8,128)(2,1)} %param.15, s32[]{:T(128)S(6)} %select_n.38, s32[192]{0:T(256)S(1)} %convert_element_type.62, s32[192]{0:T(256)S(1)} %convert_element_type.61), kind=kOutput, calls=%fused_computation.15 | convolution fusion | flops 303218688 | bytes 1967620 | tf_op jit(solution)/shard_map/dot_general | solution.py:22
  12.2 0.0 copy-done.13
  12.2 1.9 multiply_convert_fusion
  14.1 64.4 %dispatch.1 = (bf16[16,48,2048]{2,1,0:T(8,128)(2,1)}, bf16[16,48,2048]{2,1,0:T(8,128)(2,1)}) custom-call(bf16[16,48,1024]{2,1,0:T(8,128)(2,1)} %bitcast.46, bf16[16,48,1024]{2,1,0:T(8,128)(2,1)} %bitcast.44), custom_call_target="tpu_custom_call" | custom-call | flops 1000000 | bytes 100000000 | tf_op jit(solution)/shard_map/dispatch/pallas_call | solution.py:391
  78.5 0.0 copy-done
  78.5 0.0 copy-start.2
  78.5 0.0 copy-start.9
  78.5 3.8 %fusion.2 = f32[768,512]{1,0:T(8,128)S(1)} fusion(bf16[768,2048]{1,0:T(8,128)(2,1)} %bitcast.54, bf16[1,2048,512]{2,1,0:T(8,128)(2,1)S(1)} %copy-done), kind=kOutput, calls=%fused_computation.8 | convolution fusion | flops 1610612736 | bytes 6815744 | tf_op jit(solution)/shard_map/dot_general | solution.py:22
  82.3 0.0 copy-done.2
  82.4 0.0 copy-done.9
  82.4 0.0 copy-start.15
  82.4 0.0 copy-start.7
  82.4 0.0 copy-start.11
  82.4 1.8 fusion.5
  84.2 0.0 copy-start.17
  84.2 0.0 copy-done.15
  84.2 0.6 copy-done.7
  84.8 1.2 copy-done.11
  86.0 2.3 multiply_convert_fusion.2
  88.4 0.0 copy-done.17
  88.4 0.0 copy-start.3
  88.4 0.0 copy-start.5
  88.4 1.8 fusion
  90.2 0.0 copy-done.3
  90.2 0.0 copy-done.5
  90.3 3.5 %add_convert_fusion = bf16[768,2048]{1,0:T(8,128)(2,1)} fusion(f32[768,2048]{1,0:T(8,128)S(1)} %fusion, bf16[768,512]{1,0:T(8,128)(2,1)S(1)} %get-tuple-element.39, bf16[1,2048,512]{2,1,0:T(8,128)(2,1)S(1)} %copy-done.2), kind=kOutput, calls=%fused_computation | convolution fusion | flops 1613758464 | bytes 12320768 | tf_op jit(solution)/shard_map/dot_general | solution.py:22
  93.7 1.7 constant_dynamic-slice_fusion
  95.4 0.1 collective-permute-start
  95.5 3.4 %collective-permute-done = bf16[768,1024]{1,0:T(8,128)(2,1)S(1)} collective-permute-done((bf16[768,1024]{1,0:T(8,128)(2,1)S(1)}, bf16[768,1024]{1,0:T(8,128)(2,1)S(1)}, u32[]{:S(2)}, u32[]{:S(2)}) %collective-permute-start) | collective-permute-done | bytes 1572896 | tf_op jit(solution)/shard_map/ppermute | solution.py:475
  98.9 0.0 copy-done.1
  98.9 0.7 add_convert_fusion.1
  99.6 0.0 copy-start.14
  99.6 65.6 %all_to_all.5 = bf16[16,48,1024]{2,1,0:T(8,128)(2,1)S(1)} all-to-all(bf16[16,48,1024]{2,1,0:T(8,128)(2,1)S(1)} %bitcast.45), channel_id=1, replica_groups=mesh['sp'=16,'tp'=2] {'sp'}, dimensions={0} | all-to-all | bytes 3145728 | tf_op jit(solution)/shard_map/all_to_all | solution.py:477
  165.3 0.0 copy-done.14
  165.3 0.5 fusion.10
  165.8 0.1 collective-permute-start.1
  165.9 1.8 collective-permute-done.1
  167.7 1.1 broadcast_select_fusion.1
  168.8 0.0 copy-done.6
  168.8 2.7 fusion.12
  171.5 0.0 reduce-scatter.2.cloned.1.call-update
  171.5 2.7 mixer_prep.1
  174.2 24.7 %first_exchange.1 = (f32[2,64,256]{2,1,0:T(8,128)}, f32[16,8,512]{2,1,0:T(8,128)}) custom-call(bf16[2,64,256]{2,1,0:T(8,128)(2,1)} %get-tuple-element.28.x_ref, f32[8,512]{1,0:T(8,128)} %get-tuple-element.29.tot_ref), custom_call_target="tpu_custom_call" | custom-call | flops 1000000 | bytes 8000000 | tf_op jit(solution)/shard_map/first_exchange/pallas_call | solution.py:245
  198.9 0.0 copy-start.4
  198.9 0.0 copy-start.10
  198.9 6.1 %convolution_bitcast_fusion.1 = f32[1,2048,512]{2,1,0:T(8,128)} fusion(bf16[768,2048]{1,0:T(8,128)(2,1)} %bitcast.55, bf16[768,512]{1,0:T(8,128)(2,1)} %copy-done.5), kind=kOutput, calls=%fused_computation.2 | convolution fusion | flops 1610612736 | bytes 8126464 | tf_op jit(solution)/shard_map/dot_general | solution.py:22
  205.0 0.0 copy-done.4
  205.0 0.0 copy-done.10
  205.0 0.0 copy-start.16
  205.0 3.9 %convolution_bitcast_fusion.2 = f32[1,2048,512]{2,1,0:T(8,128)} fusion(bf16[768,2048]{1,0:T(8,128)(2,1)S(1)} %bitcast.57, bf16[768,512]{1,0:T(8,128)(2,1)S(1)} %copy-done.4), kind=kOutput, calls=%fused_computation.3 | convolution fusion | flops 1610612736 | bytes 8126464 | tf_op jit(solution)/shard_map/dot_general | solution.py:22
  209.0 0.0 copy-done.16
  209.0 4.0 %convolution_bitcast_fusion = f32[1,512,2048]{2,1,0:T(8,128)} fusion(bf16[768,2048]{1,0:T(8,128)(2,1)S(1)} %bitcast.53, f32[768,512]{1,0:T(8,128)S(1)} %copy-done.18, f32[768,512]{1,0:T(8,128)S(1)} %copy-done.16), kind=kOutput, calls=%fused_computation.1 | convolution fusion | flops 1612972032 | bytes 10485760 | tf_op jit(solution)/shard_map/dot_general | solution.py:22
  213.0 1.3 convolution_convert_fusion.1.do_ref
  214.2 2.1 mixer_pull.1.x_ref
  216.4 24.8 %second_exchange.1.leave_ref = f32[2,64,256]{2,1,0:T(8,128)} custom-call(bf16[2,64,256]{2,1,0:T(8,128)(2,1)} %mixer_pull.1.x_ref, f32[16,8,512]{2,1,0:T(8,128)} %get-tuple-element.31.totals_ref), custom_call_target="tpu_custom_call" | custom-call | flops 1000000 | bytes 8000000 | tf_op jit(solution)/shard_map/second_exchange/pallas_call | solution.py:274
  241.2 5.6 %mixer_grads.1 = (f32[192,256]{1,0:T(8,128)}, f32[192,256]{1,0:T(8,128)}, f32[192,512]{1,0:T(8,128)}, f32[192,256]{1,0:T(8,128)}, f32[192,256]{1,0:T(8,128)}) custom-call(bf16[192,256]{1,0:T(8,128)(2,1)} %q_ref.3, bf16[192,256]{1,0:T(8,128)(2,1)} %k_ref.3, bf16[192,512]{1,0:T(8,128)(2,1)} %v_ref.3, bf16[192,512]{1,0:T(8,128)(2,1)} %convolution_convert_fusion.1.do_ref, ...), custom_call_target="tpu_custom_call" | custom-call | flops 8000000000 | bytes 4000000 | tf_op jit(solution)/shard_map/mixer_grads/pallas_call | solution.py:286
  246.8 32.8 %reduce-scatter.2.cloned.1.call-done = f32[128,512]{1,0:T(8,128)} async-done(((f32[2048,512]{1,0:T(8,128)}), f32[128,512]{1,0:T(8,128)}) %reduce-scatter.2.cloned.1.call-update) | async-done | bytes 262160 | tf_op jit(solution)/shard_map/reduce_scatter | solution.py:490
  (11 shorter events, 0.0 us)
Async XLA Ops:
  7.2 71.3 %copy-start = (bf16[1,2048,512]{2,1,0:T(8,128)(2,1)S(1)}, bf16[1,2048,512]{2,1,0:T(8,128)(2,1)}, u32[]{:S(2)}) copy-start(bf16[1,2048,512]{2,1,0:T(8,128)(2,1)} %param.18) | copy-start | bytes 6291460
  7.2 5.0 %copy-start.13 = (bf16[192,2048]{1,0:T(8,128)(2,1)S(1)}, bf16[192,2048]{1,0:T(8,128)(2,1)}, u32[]{:S(2)}) copy-start(bf16[192,2048]{1,0:T(8,128)(2,1)} %param.14) | copy-start | bytes 2359300
  7.2 272.5 %reduce-scatter.2.cloned.1.call-start = ((), (), s32[]{:S(2)}) async-start(), calls=%async_computation.2 | async-start | bytes 4456448 | tf_op jit(solution)/shard_map/reduce_scatter | solution.py:490
  78.5 3.8 %copy-start.2 = (bf16[1,2048,512]{2,1,0:T(8,128)(2,1)S(1)}, bf16[1,2048,512]{2,1,0:T(8,128)(2,1)}, u32[]{:S(2)}) copy-start(bf16[1,2048,512]{2,1,0:T(8,128)(2,1)} %param.19) | copy-start | bytes 6291460
  78.5 3.8 %copy-start.9 = (bf16[16,48,2048]{2,1,0:T(8,128)(2,1)S(1)}, bf16[16,48,2048]{2,1,0:T(8,128)(2,1)}, u32[]{:S(2)}) copy-start(bf16[16,48,2048]{2,1,0:T(8,128)(2,1)} %get-tuple-element.23) | copy-start | bytes 9437188
  82.4 1.8 copy-start.15
  82.4 2.5 copy-start.7
  82.4 3.7 %copy-start.11 = (bf16[1,512,2048]{2,1,0:T(8,128)(2,1)S(1)}, bf16[1,512,2048]{2,1,0:T(8,128)(2,1)}, u32[]{:S(2)}) copy-start(bf16[1,512,2048]{2,1,0:T(8,128)(2,1)} %param.20) | copy-start | bytes 6291460
  84.2 4.2 %copy-start.17 = (f32[768,512]{1,0:T(8,128)}, f32[768,512]{1,0:T(8,128)S(1)}, u32[]{:S(2)}) copy-start(f32[768,512]{1,0:T(8,128)S(1)} %fusion.5) | copy-start | bytes 4718596
  88.4 1.9 copy-start.3
  88.4 1.9 copy-start.5
  93.7 5.2 %copy-start.1 = (bf16[768,2048]{1,0:T(8,128)(2,1)S(1)}, bf16[768,2048]{1,0:T(8,128)(2,1)}, u32[]{:S(2)}) copy-start(bf16[768,2048]{1,0:T(8,128)(2,1)} %add_convert_fusion) | copy-start | bytes 9437188
  95.4 3.5 %collective-permute-start = (bf16[768,1024]{1,0:T(8,128)(2,1)S(1)}, bf16[768,1024]{1,0:T(8,128)(2,1)S(1)}, u32[]{:S(2)}, u32[]{:S(2)}) collective-permute-start(bf16[768,1024]{1,0:T(8,128)(2,1)S(1)} %constant_dynamic-slice_fusion), channel_id=1, source_target_pairs={{0,1},{1,0},{2,3},{3,2},{4,5},{5,4},{6,7},{7,6},{8,9},{9,8},{10,11... | collective-permute-start | bytes 4718600 | tf_op jit(solution)/shard_map/ppermute | solution.py:475
  99.6 65.7 %copy-start.14 = (bf16[192,2048]{1,0:T(8,128)(2,1)S(1)}, bf16[192,2048]{1,0:T(8,128)(2,1)}, u32[]{:S(2)}) copy-start(bf16[192,2048]{1,0:T(8,128)(2,1)} %param.14) | copy-start | bytes 2359300
  165.3 3.5 %copy-start.6 = (bf16[192,512]{1,0:T(8,128)(2,1)S(1)}, bf16[192,512]{1,0:T(8,128)(2,1)}, u32[]{:S(2)}) copy-start(bf16[192,512]{1,0:T(8,128)(2,1)} %param.22) | copy-start | bytes 589828
  165.8 1.9 collective-permute-start.1
  198.9 6.1 %copy-start.4 = (bf16[768,512]{1,0:T(8,128)(2,1)S(1)}, bf16[768,512]{1,0:T(8,128)(2,1)}, u32[]{:S(2)}) copy-start(bf16[768,512]{1,0:T(8,128)(2,1)} %copy-done.3) | copy-start | bytes 2359300
  198.9 6.1 %copy-start.10 = (bf16[16,48,2048]{2,1,0:T(8,128)(2,1)S(1)}, bf16[16,48,2048]{2,1,0:T(8,128)(2,1)}, u32[]{:S(2)}) copy-start(bf16[16,48,2048]{2,1,0:T(8,128)(2,1)} %get-tuple-element.23) | copy-start | bytes 9437188
  205.0 3.9 %copy-start.8 = (bf16[16,48,2048]{2,1,0:T(8,128)(2,1)S(1)}, bf16[16,48,2048]{2,1,0:T(8,128)(2,1)}, u32[]{:S(2)}) copy-start(bf16[16,48,2048]{2,1,0:T(8,128)(2,1)} %get-tuple-element.24) | copy-start | bytes 9437188
  205.0 3.9 %copy-start.16 = (f32[768,512]{1,0:T(8,128)S(1)}, f32[768,512]{1,0:T(8,128)}, u32[]{:S(2)}) copy-start(f32[768,512]{1,0:T(8,128)} %copy-done.15) | copy-start | bytes 4718596
  205.0 3.9 %copy-start.18 = (f32[768,512]{1,0:T(8,128)S(1)}, f32[768,512]{1,0:T(8,128)}, u32[]{:S(2)}) copy-start(f32[768,512]{1,0:T(8,128)} %copy-done.17) | copy-start | bytes 4718596
  209.0 4.0 %copy-start.12 = (bf16[2048,512]{1,0:T(8,128)(2,1)S(1)}, bf16[2048,512]{1,0:T(8,128)(2,1)}, u32[]{:S(2)}) copy-start(bf16[2048,512]{1,0:T(8,128)(2,1)} %param.21) | copy-start | bytes 6291460
Sparse Core Ops, SparseCore 0:
  171.6 107.9 reduce-scatter.1

commit v2 on v1

--- a/solution.py
+++ b/solution.py
@@ -401,6 +401,37 @@
     )(routed_cot, routed_tok)
 
 
+def return_kernel(count, source, result, send, recv, own_sem):
+    me = lax.axis_index("sp")
+    own = pltpu.make_async_copy(source.at[me], result.at[me], own_sem)
+    own.start()
+
+    def make(step, target, half):
+        return (
+            pltpu.make_async_remote_copy(
+                src_ref=source.at[target], dst_ref=result.at[me], send_sem=send.at[step],
+                recv_sem=recv.at[step], device_id={"sp": target}, device_id_type=MESH,
+            ),
+        )
+
+    send_all(count, me, make)
+    own.wait()
+
+
+def send_back(rows):
+    groups = rows.shape[0]
+    return pl.pallas_call(
+        functools.partial(return_kernel, groups),
+        out_shape=shaped(rows.shape, BF16),
+        in_specs=[ANY],
+        out_specs=ANY,
+        scratch_shapes=[pltpu.SemaphoreType.DMA((groups,))] * 2 + [pltpu.SemaphoreType.DMA],
+        compiler_params=pltpu.CompilerParams(collective_id=4, has_side_effects=True),
+        cost_estimate=cost(10**6, 5 * 10**7),
+        name="send_back",
+    )(rows)
+
+
 def local(
     cotangent,
     mixed_input,
@@ -450,10 +481,11 @@
     own_tok = lax.dynamic_slice_in_dim(mixed_input, core * half, half, 1)
     routed_cot = (slot_gate * dot(pick, own_cot)).astype(BF16)
     routed_tok = dot(pick, own_tok).astype(BF16)
+    started = mixer_start(key_rows, value_rows, log_forward, log_backward)
+    routed_cot, routed_tok, started = lax.optimization_barrier((routed_cot, routed_tok, started))
     cot_in, tok_in = dispatch(
         routed_cot.reshape(groups, slot_count, half), routed_tok.reshape(groups, slot_count, half)
     )
-    started = mixer_start(key_rows, value_rows, log_forward, log_backward)
     w_gate = expert_gate[0]
     w_up = expert_up[0]
     w_down = expert_down[0]
@@ -474,9 +506,7 @@
     other = lax.dynamic_slice_in_dim(partial_value, (1 - core) * half, half, 1)
     came = lax.ppermute(other, "tp", swap)
     summed = (mine.astype(F32) + came.astype(F32)).astype(BF16)
-    returned = lax.all_to_all(
-        summed.reshape(groups, slot_count, half), "sp", split_axis=0, concat_axis=0, tiled=True
-    ).reshape(row_total, half)
+    returned = send_back(summed.reshape(groups, slot_count, half)).reshape(row_total, half)
     down_term = dot(hidden, cot_block, contract_first)
     gate_term = dot(tok_block, gate_pre_grad, contract_first)
     up_term = dot(tok_block, up_pre_grad, contract_first)

time: 287 us -> 304 us (1.059)
  blocking collectives: 65.6 us -> 0 us
  Pallas kernels: 124 us -> 178 us
  waiting for transfers between devices: 38.1 us -> 64.3 us
    all_to_all x1 -> x0, blocking collectives: 65.6 us -> none  [local(): lax.all_to_all(summed.reshape(groups, slot_count, half), 'sp', split_axis...]
    pallas_call x0 -> x1, Pallas kernels: none -> 55.6 us  [send_back(): pl.pallas_call(functools.partial(return_kernel, groups), out_shape=shaped...]
    reduce_scatter x1, waiting for transfers between devices: 32.8 us -> 59.1 us  [local(): lax.psum_scatter(dot(mid_grad, mixer_output, contract_first), 'sp', scatt...]
    pallas_call x1, Pallas kernels: 24.8 us -> 29.5 us  [mixer_grads(): pl.pallas_call(functools.partial(second_exchange, groups), out_shape=shap...]
    pallas_call x1, Pallas kernels: 64.4 us -> 60.5 us  [dispatch(): pl.pallas_call(functools.partial(dispatch_kernel, groups), out_shape=(who...]
  transfers between devices with their start and end apart: 3 -> 3, of which waited for: 3 -> 3; matrix products, arithmetic and copies ran while one was open for 5% -> 5% of each run, Pallas kernels for 21% -> 12%
where the time goes in v2:
time: 304 us; the launch traced here: 303 us
  Pallas kernels  178 us (59%)
  waiting for transfers between devices  64.3 us (21%)
  matrix products  38.1 us (13%)
  between operations  14.4 us (5%)
  local copies, waits for them, and re-layouts  5.27 us (2%)
  other arithmetic  3.1 us (1%)
    pallas_call x1, Pallas kernels, dispatch(): pl.pallas_call(functools.partial(dispatch_kernel, groups), out_shape=(who...  60.5 us
    reduce_scatter x1, waiting for transfers between devices, local(): lax.psum_scatter(dot(mid_grad, mixer_output, contract_first), 'sp', scatt...  59.1 us
    pallas_call x1, Pallas kernels, send_back(): pl.pallas_call(functools.partial(return_kernel, groups), out_shape=shaped...  55.6 us
    dot_general x14, matrix products, dot(): lax.dot_general(a, b, (dims, ((), ())), preferred_element_type=F32, preci...  38.1 us
    pallas_call x1, Pallas kernels, mixer_grads(): pl.pallas_call(functools.partial(second_exchange, groups), out_shape=shap...  29.5 us
    pallas_call x1, Pallas kernels, mixer_start(): pl.pallas_call(functools.partial(first_exchange, groups), out_shape=(shap...  22 us
  transfers between devices with their start and end apart: 3, of which 3 were waited for; matrix products, arithmetic and copies ran while one was open for 5% of the time, Pallas kernels for 12%

profile of v2, /device:TPU:0, one launch (start us, length us, event | category | flops | bytes accessed | tf_op | source)
XLA Modules:
  0.0 303.4 jit_solution(6156594881112735802)
XLA Ops:
  7.2 0.0 copy-start
  7.2 0.0 copy-start.13
  7.2 0.0 reduce-scatter.2.cloned.1.call-start
  7.3 0.9 fusion.35
  8.2 0.2 select_reduce_fusion.1
  8.4 0.8 fusion.34
  9.1 0.2 add_reduce_fusion
  9.3 2.9 convolution_convert_fusion
  12.2 0.0 copy-done.13
  12.2 1.9 multiply_convert_fusion
  14.1 2.7 mixer_prep.1
  16.8 22.0 %first_exchange.1 = (f32[2,64,256]{2,1,0:T(8,128)}, f32[16,8,512]{2,1,0:T(8,128)}) custom-call(bf16[2,64,256]{2,1,0:T(8,128)(2,1)} %get-tuple-element.33.x_ref, f32[8,512]{1,0:T(8,128)} %get-tuple-element.34.tot_ref), custom_call_target="tpu_custom_call" | custom-call | flops 1000000 | bytes 8000000 | tf_op jit(solution)/shard_map/first_exchange/pallas_call | solution.py:245
  38.7 60.5 %dispatch.1 = (bf16[16,48,2048]{2,1,0:T(8,128)(2,1)}, bf16[16,48,2048]{2,1,0:T(8,128)(2,1)}) custom-call(bf16[16,48,1024]{2,1,0:T(8,128)(2,1)} %bitcast.46, bf16[16,48,1024]{2,1,0:T(8,128)(2,1)} %bitcast.44), custom_call_target="tpu_custom_call" | custom-call | flops 1000000 | bytes 100000000 | tf_op jit(solution)/shard_map/dispatch/pallas_call | solution.py:391
  99.3 0.0 copy-done
  99.3 0.0 copy-start.2
  99.3 0.0 copy-start.9
  99.3 3.8 %fusion.2 = f32[768,512]{1,0:T(8,128)S(1)} fusion(bf16[768,2048]{1,0:T(8,128)(2,1)} %bitcast.54, bf16[1,2048,512]{2,1,0:T(8,128)(2,1)S(1)} %copy-done), kind=kOutput, calls=%fused_computation.8 | convolution fusion | flops 1610612736 | bytes 6815744 | tf_op jit(solution)/shard_map/dot_general | solution.py:22
  103.1 0.0 copy-done.2
  103.1 0.0 copy-done.9
  103.1 0.0 copy-start.14
  103.1 0.0 copy-start.7
  103.2 0.0 copy-start.11
  103.2 1.8 fusion.5
  105.0 0.0 copy-start.16
  105.0 0.0 copy-done.14
  105.0 0.6 copy-done.7
  105.6 1.2 copy-done.11
  106.8 2.3 multiply_convert_fusion.2
  109.1 0.0 copy-done.16
  109.2 0.0 copy-start.3
  109.2 0.0 copy-start.5
  109.2 1.8 fusion
  111.0 0.0 copy-done.3
  111.0 0.0 copy-done.5
  111.0 3.5 %add_convert_fusion = bf16[768,2048]{1,0:T(8,128)(2,1)} fusion(f32[768,2048]{1,0:T(8,128)S(1)} %fusion, bf16[768,512]{1,0:T(8,128)(2,1)S(1)} %get-tuple-element.53, bf16[1,2048,512]{2,1,0:T(8,128)(2,1)S(1)} %copy-done.2), kind=kOutput, calls=%fused_computation | convolution fusion | flops 1613758464 | bytes 12320768 | tf_op jit(solution)/shard_map/dot_general | solution.py:22
  114.5 1.7 constant_dynamic-slice_fusion
  116.2 0.1 collective-permute-start
  116.3 3.4 %collective-permute-done = bf16[768,1024]{1,0:T(8,128)(2,1)S(1)} collective-permute-done((bf16[768,1024]{1,0:T(8,128)(2,1)S(1)}, bf16[768,1024]{1,0:T(8,128)(2,1)S(1)}, u32[]{:S(2)}, u32[]{:S(2)}) %collective-permute-start) | collective-permute-done | bytes 1572896 | tf_op jit(solution)/shard_map/ppermute | solution.py:507
  119.7 0.0 copy-done.1
  119.7 1.8 add_convert_fusion.1
  121.5 55.6 %send_back.1 = bf16[16,48,1024]{2,1,0:T(8,128)(2,1)} custom-call(bf16[16,48,1024]{2,1,0:T(8,128)(2,1)} %bitcast.45), custom_call_target="tpu_custom_call" | custom-call | flops 1000000 | bytes 50000000 | tf_op jit(solution)/shard_map/send_back/pallas_call | solution.py:423
  177.2 0.0 copy-start.6
  177.2 2.0 fusion.10
  179.2 0.1 collective-permute-start.1
  179.3 1.8 collective-permute-done.1
  181.1 1.1 broadcast_select_fusion.1
  182.2 0.0 copy-done.6
  182.2 2.7 fusion.12
  184.9 0.0 reduce-scatter.2.cloned.1.call-update
  184.9 0.0 copy-start.4
  184.9 0.0 copy-start.10
  184.9 6.1 %convolution_bitcast_fusion.1 = f32[1,2048,512]{2,1,0:T(8,128)} fusion(bf16[768,2048]{1,0:T(8,128)(2,1)} %bitcast.55, bf16[768,512]{1,0:T(8,128)(2,1)} %copy-done.5), kind=kOutput, calls=%fused_computation.2 | convolution fusion | flops 1610612736 | bytes 8126464 | tf_op jit(solution)/shard_map/dot_general | solution.py:22
  191.0 0.0 copy-done.4
  191.0 0.0 copy-done.10
  191.0 0.0 copy-start.15
  191.0 0.0 copy-start.17
  191.1 3.9 %convolution_bitcast_fusion.2 = f32[1,2048,512]{2,1,0:T(8,128)} fusion(bf16[768,2048]{1,0:T(8,128)(2,1)S(1)} %bitcast.57, bf16[768,512]{1,0:T(8,128)(2,1)S(1)} %copy-done.4), kind=kOutput, calls=%fused_computation.3 | convolution fusion | flops 1610612736 | bytes 8126464 | tf_op jit(solution)/shard_map/dot_general | solution.py:22
  195.0 0.0 copy-done.8
  195.0 4.0 %convolution_bitcast_fusion = f32[1,512,2048]{2,1,0:T(8,128)} fusion(bf16[768,2048]{1,0:T(8,128)(2,1)S(1)} %bitcast.53, f32[768,512]{1,0:T(8,128)S(1)} %copy-done.17, f32[768,512]{1,0:T(8,128)S(1)} %copy-done.15), kind=kOutput, calls=%fused_computation.1 | convolution fusion | flops 1612972032 | bytes 10485760 | tf_op jit(solution)/shard_map/dot_general | solution.py:22
  199.0 1.2 convolution_convert_fusion.1.do_ref
  200.2 2.1 mixer_pull.1.x_ref
  202.4 29.5 %second_exchange.1.leave_ref = f32[2,64,256]{2,1,0:T(8,128)} custom-call(bf16[2,64,256]{2,1,0:T(8,128)(2,1)} %mixer_pull.1.x_ref, f32[16,8,512]{2,1,0:T(8,128)} %get-tuple-element.45.totals_ref), custom_call_target="tpu_custom_call" | custom-call | flops 1000000 | bytes 8000000 | tf_op jit(solution)/shard_map/second_exchange/pallas_call | solution.py:274
  231.9 5.6 %mixer_grads.1 = (f32[192,256]{1,0:T(8,128)}, f32[192,256]{1,0:T(8,128)}, f32[192,512]{1,0:T(8,128)}, f32[192,256]{1,0:T(8,128)}, f32[192,256]{1,0:T(8,128)}) custom-call(bf16[192,256]{1,0:T(8,128)(2,1)} %q_ref.3, bf16[192,256]{1,0:T(8,128)(2,1)} %k_ref.3, bf16[192,512]{1,0:T(8,128)(2,1)} %v_ref.3, bf16[192,512]{1,0:T(8,128)(2,1)} %convolution_convert_fusion.1.do_ref, ...), custom_call_target="tpu_custom_call" | custom-call | flops 8000000000 | bytes 4000000 | tf_op jit(solution)/shard_map/mixer_grads/pallas_call | solution.py:286
  237.5 59.1 %reduce-scatter.2.cloned.1.call-done = f32[128,512]{1,0:T(8,128)} async-done(((f32[2048,512]{1,0:T(8,128)}), f32[128,512]{1,0:T(8,128)}) %reduce-scatter.2.cloned.1.call-update) | async-done | bytes 262160 | tf_op jit(solution)/shard_map/reduce_scatter | solution.py:520
  (9 shorter events, 0.0 us)
Async XLA Ops:
  7.2 92.1 %copy-start = (bf16[1,2048,512]{2,1,0:T(8,128)(2,1)S(1)}, bf16[1,2048,512]{2,1,0:T(8,128)(2,1)}, u32[]{:S(2)}) copy-start(bf16[1,2048,512]{2,1,0:T(8,128)(2,1)} %param.18) | copy-start | bytes 6291460
  7.2 5.0 %copy-start.13 = (bf16[192,2048]{1,0:T(8,128)(2,1)S(1)}, bf16[192,2048]{1,0:T(8,128)(2,1)}, u32[]{:S(2)}) copy-start(bf16[192,2048]{1,0:T(8,128)(2,1)} %param.14) | copy-start | bytes 2359300
  7.2 289.4 %reduce-scatter.2.cloned.1.call-start = ((), (), s32[]{:S(2)}) async-start(), calls=%async_computation.1 | async-start | bytes 4456448 | tf_op jit(solution)/shard_map/reduce_scatter | solution.py:520
  99.3 3.9 %copy-start.2 = (bf16[1,2048,512]{2,1,0:T(8,128)(2,1)S(1)}, bf16[1,2048,512]{2,1,0:T(8,128)(2,1)}, u32[]{:S(2)}) copy-start(bf16[1,2048,512]{2,1,0:T(8,128)(2,1)} %param.19) | copy-start | bytes 6291460
  99.3 3.8 %copy-start.9 = (bf16[16,48,2048]{2,1,0:T(8,128)(2,1)S(1)}, bf16[16,48,2048]{2,1,0:T(8,128)(2,1)}, u32[]{:S(2)}) copy-start(bf16[16,48,2048]{2,1,0:T(8,128)(2,1)} %get-tuple-element.39) | copy-start | bytes 9437188
  103.1 1.8 copy-start.14
  103.1 2.5 copy-start.7
  103.2 3.7 %copy-start.11 = (bf16[1,512,2048]{2,1,0:T(8,128)(2,1)S(1)}, bf16[1,512,2048]{2,1,0:T(8,128)(2,1)}, u32[]{:S(2)}) copy-start(bf16[1,512,2048]{2,1,0:T(8,128)(2,1)} %param.20) | copy-start | bytes 6291460
  105.0 4.2 %copy-start.16 = (f32[768,512]{1,0:T(8,128)}, f32[768,512]{1,0:T(8,128)S(1)}, u32[]{:S(2)}) copy-start(f32[768,512]{1,0:T(8,128)S(1)} %fusion.5) | copy-start | bytes 4718596
  109.2 1.9 copy-start.3
  109.2 1.9 copy-start.5
  114.5 5.2 %copy-start.1 = (bf16[768,2048]{1,0:T(8,128)(2,1)S(1)}, bf16[768,2048]{1,0:T(8,128)(2,1)}, u32[]{:S(2)}) copy-start(bf16[768,2048]{1,0:T(8,128)(2,1)} %add_convert_fusion) | copy-start | bytes 9437188
  116.2 3.5 %collective-permute-start = (bf16[768,1024]{1,0:T(8,128)(2,1)S(1)}, bf16[768,1024]{1,0:T(8,128)(2,1)S(1)}, u32[]{:S(2)}, u32[]{:S(2)}) collective-permute-start(bf16[768,1024]{1,0:T(8,128)(2,1)S(1)} %constant_dynamic-slice_fusion), channel_id=1, source_target_pairs={{0,1},{1,0},{2,3},{3,2},{4,5},{5,4},{6,7},{7,6},{8,9},{9,8},{10,11... | collective-permute-start | bytes 4718600 | tf_op jit(solution)/shard_map/ppermute | solution.py:507
  177.2 5.0 %copy-start.6 = (bf16[192,512]{1,0:T(8,128)(2,1)S(1)}, bf16[192,512]{1,0:T(8,128)(2,1)}, u32[]{:S(2)}) copy-start(bf16[192,512]{1,0:T(8,128)(2,1)} %param.22) | copy-start | bytes 589828
  179.2 1.9 collective-permute-start.1
  184.9 6.1 %copy-start.4 = (bf16[768,512]{1,0:T(8,128)(2,1)S(1)}, bf16[768,512]{1,0:T(8,128)(2,1)}, u32[]{:S(2)}) copy-start(bf16[768,512]{1,0:T(8,128)(2,1)} %copy-done.3) | copy-start | bytes 2359300
  184.9 6.1 %copy-start.10 = (bf16[16,48,2048]{2,1,0:T(8,128)(2,1)S(1)}, bf16[16,48,2048]{2,1,0:T(8,128)(2,1)}, u32[]{:S(2)}) copy-start(bf16[16,48,2048]{2,1,0:T(8,128)(2,1)} %get-tuple-element.39) | copy-start | bytes 9437188
  191.0 3.9 %copy-start.8 = (bf16[16,48,2048]{2,1,0:T(8,128)(2,1)S(1)}, bf16[16,48,2048]{2,1,0:T(8,128)(2,1)}, u32[]{:S(2)}) copy-start(bf16[16,48,2048]{2,1,0:T(8,128)(2,1)} %get-tuple-element.40) | copy-start | bytes 9437188
  191.0 3.9 %copy-start.15 = (f32[768,512]{1,0:T(8,128)S(1)}, f32[768,512]{1,0:T(8,128)}, u32[]{:S(2)}) copy-start(f32[768,512]{1,0:T(8,128)} %copy-done.14) | copy-start | bytes 4718596
  191.0 3.9 %copy-start.17 = (f32[768,512]{1,0:T(8,128)S(1)}, f32[768,512]{1,0:T(8,128)}, u32[]{:S(2)}) copy-start(f32[768,512]{1,0:T(8,128)} %copy-done.16) | copy-start | bytes 4718596
  195.0 4.0 %copy-start.12 = (bf16[2048,512]{1,0:T(8,128)(2,1)S(1)}, bf16[2048,512]{1,0:T(8,128)(2,1)}, u32[]{:S(2)}) copy-start(bf16[2048,512]{1,0:T(8,128)(2,1)} %param.21) | copy-start | bytes 6291460
Sparse Core Ops, SparseCore 0:
  185.0 111.4 reduce-scatter.1
